TPU v7x, 512 devices: a whole 4x4x16 slice. The times are simulated.
512 devices in a mesh: sp: 64 (over z, y), tp: 8 (over x, core).
Axes of the slice: x: 4, y: 4, z: 16, core: 2. Of those that a mesh axis runs over, the one named last changes fastest.
Arguments:
- queries: bfloat16 [8192, 1024], P('sp', 'tp'), may hold values from -6 to 6
- attn_out: bfloat16 [8192, 1024], P('sp', 'tp'), may hold values from -6 to 6
- out_grad: bfloat16 [8192, 1024], P('sp', 'tp'), may hold values from -384 to 384
- row_lse: float32 [8192, 8], P('sp', 'tp'), may hold values from 9.5 to 12.5
- source: bfloat16 [32768, 4096], P('sp', 'tp'), may hold values from -6 to 6
- saved_keys: bfloat16 [32768, 256], P('sp'), may hold values from -6 to 6
- saved_values: bfloat16 [32768, 256], P('sp'), may hold values from -6 to 6
- key_weight: bfloat16 [4096, 256], P('tp'), may hold values from -0.09375 to 0.09375
- value_weight: bfloat16 [4096, 256], P('tp'), may hold values from -0.09375 to 0.09375
Outputs:
- query_grad: float32 [8192, 1024], P('sp', 'tp')
- source_grad: float32 [32768, 4096], P('sp', 'tp')
- key_grad: float32 [256, 4096], P('sp', 'tp')
All inputs are finite; a program needn't handle non-finite values.
Results may differ from a plain program's by a relative error of at most 0.012.
Values may be sent and summed in bfloat16 or wider, within the bound.
A program may use at most 64 MiB of HBM per device.

v0:
```python
import functools
import math

import jax
import jax.numpy as jnp
from jax import lax
from jax.experimental import pallas as pl
from jax.experimental.pallas import tpu as pltpu
from jax.sharding import PartitionSpec as P

HEADS = 8
KV_HEADS = 2
HEAD_DIM = 128
LOG2E = 1.0 / math.log(2.0)
MESH = pl.DeviceIdType.MESH
F32 = jnp.float32
BF16 = jnp.bfloat16


def dot_nt(left, right, precision=None):
    return lax.dot_general(
        left, right, (((1,), (1,)), ((), ())), preferred_element_type=F32, precision=precision
    )


def dot_tn(left, right):
    return lax.dot_general(left, right, (((0,), (0,)), ((), ())), preferred_element_type=F32)


def dot_nn(left, right):
    return jnp.dot(left, right, preferred_element_type=F32)


def kernel(
    tgt_n, src_n, key_n, tp_n, src_total,
    q_ref, o_ref, d_ref, lse_ref, key_ref, value_ref, source_ref,
    dq_ref, kv_ref, kg_ref,
    qd, stats, kvs, dk, dv, dq_acc, dq_out, dq_in, dq_via, g_out, g_in, tp_own, tp_in,
    src, a_out, a_in, a2_own, a2_out, a2_in, b_out, b_in, b2_own, b2_out, b2_in,
    copy_sem, qd_s, qd_r, rq_s, st_s, st_r, kv_s, kv_r, rkv_s, dq_s, dq_r, via_r, g_s, g_r, tp_s, tp_r,
    a_s, a_r, a2_s, a2_r, b_s, b_r, b2_s, b2_r,
):
    sp = lax.axis_index("sp")
    tp = lax.axis_index("tp")
    sp_n = tgt_n * src_n
    t_hi, t_lo = sp // (2 * src_n), sp % 2
    me_t = t_hi * 2 + t_lo
    me_s = (sp // 2) % src_n
    s_hi, s_lo = me_s // 2, me_s % 2
    near_t, near_s = t_hi * 2 + 1 - t_lo, s_hi * 2 + 1 - s_lo
    t_his = [lax.rem(t_hi + k, tgt_n // 2) for k in range(1, tgt_n // 2)]
    s_his = [lax.rem(s_hi + k, src_n // 2) for k in range(1, src_n // 2)]
    far_t = [hi * 2 + t_lo for hi in t_his]
    diag_t = [hi * 2 + 1 - t_lo for hi in t_his]
    far_s = [hi * 2 + s_lo for hi in s_his]
    diag_s = [hi * 2 + 1 - s_lo for hi in s_his]
    t_peers = far_t + [near_t] + diag_t
    s_peers = far_s + [near_s] + diag_s
    key_m = sp_n // key_n
    me_o, me_i = sp // key_n, sp % key_n
    o_peers = [lax.rem(me_o + k, key_m) for k in range(1, key_m)]
    i_peers = [lax.rem(me_i + k, key_n) for k in range(1, key_n)]
    tp_peers = [lax.rem(tp + k, tp_n) for k in range(1, tp_n)]
    rows = q_ref.shape[0]
    heads = q_ref.shape[1] // HEAD_DIM
    chunks = stats.shape[1]
    per_chunk = heads // chunks
    src_rows = key_ref.shape[0]
    per_key = HEADS // KV_HEADS
    scale = 1.0 / math.sqrt(HEAD_DIM)
    kv_col = pl.multiple_of(tp * heads // per_key * HEAD_DIM, HEAD_DIM)

    def t_dev(t):
        return {"sp": t // 2 * (2 * src_n) + me_s * 2 + t % 2, "tp": tp}

    def s_dev(s):
        return {"sp": t_hi * (2 * src_n) + s * 2 + t_lo, "tp": tp}

    def o_dev(o):
        return {"sp": o * key_n + me_i, "tp": tp}

    def i_dev(i):
        return {"sp": me_o * key_n + i, "tp": tp}

    def tp_dev(p):
        return {"sp": sp, "tp": p}

    def remote(source, target, send, recv, device):
        return pltpu.make_async_remote_copy(
            src_ref=source, dst_ref=target, send_sem=send, recv_sem=recv,
            device_id=device, device_id_type=MESH,
        )

    load = pltpu.make_async_copy(source_ref, src, copy_sem)
    load.start()
    barrier = pltpu.get_barrier_semaphore()
    for k in range(1, sp_n):
        pl.semaphore_signal(
            barrier, inc=1, device_id={"sp": lax.rem(sp + k, sp_n), "tp": tp}, device_id_type=MESH
        )
    for p in tp_peers:
        pl.semaphore_signal(barrier, inc=1, device_id=tp_dev(p), device_id_type=MESH)
    ones = jnp.ones((8, HEAD_DIM), F32)
    for h in range(heads):
        cols = pl.ds(h * HEAD_DIM, HEAD_DIM)
        c, span = h // per_chunk, pl.ds(h % per_chunk * rows, rows)
        prod = d_ref[:, cols].astype(F32) * o_ref[:, cols].astype(F32)
        delta = dot_nt(ones, prod, lax.Precision.HIGHEST)
        stats[me_t, c, 0:1, span] = lse_ref[h : h + 1, :] * LOG2E
        stats[me_t, c, 1:2, span] = delta[0:1, :]
    kvs[me_s, 0] = key_ref[:, pl.ds(kv_col, HEAD_DIM)]
    kvs[me_s, 1] = value_ref[:, pl.ds(kv_col, HEAD_DIM)]
    qd[me_t, 0] = q_ref[...]
    qd[me_t, 1] = d_ref[...]
    dk[...] = jnp.zeros_like(dk)
    dv[...] = jnp.zeros_like(dv)
    dq_acc[...] = jnp.zeros_like(dq_acc)
    pl.semaphore_wait(barrier, sp_n + tp_n - 2)

    def send_q(t):
        for i, ref in enumerate((q_ref, d_ref)):
            remote(ref, qd.at[me_t, i], qd_s.at[t, i], qd_r.at[me_t, i], t_dev(t)).start()

    for s in far_s + [near_s]:
        remote(kvs.at[me_s], kvs.at[me_s], kv_s.at[s], kv_r.at[me_s], s_dev(s)).start()
    for t in far_t + [near_t]:
        send_q(t)

    for t in t_peers:
        remote(stats.at[me_t], stats.at[me_t], st_s.at[t], st_r.at[me_t], t_dev(t)).start()

    def stack(t, i, c):
        low = c * per_chunk
        return jnp.concatenate(
            [
                qd[t, i, :, pl.ds(pl.multiple_of((low + h) * HEAD_DIM, HEAD_DIM), HEAD_DIM)]
                for h in range(per_chunk)
            ],
            axis=0,
        )

    def tile(t, s):
        def body(c, carry):
            q, d = stack(t, 0, c), stack(t, 1, c)
            k, v = kvs[s, 0], kvs[s, 1]
            scores = dot_nt(k, q)
            probs = jnp.exp2(scores * (scale * LOG2E) - stats[t, c, 0:1, :])
            dprobs = dot_nt(v, d)
            dscores = (probs * (dprobs - stats[t, c, 1:2, :])).astype(BF16)
            dv[s] += dot_nn(probs.astype(BF16), d)
            dk[s] += dot_nn(dscores, q)
            dq_acc[t, c] += dot_tn(dscores, k)
            return carry

        lax.fori_loop(0, chunks, body, 0)

    def got_q(t, c):
        remote(qd.at[t, c], qd.at[t, c], qd_s.at[t, c], qd_r.at[t, c], t_dev(t)).wait_recv()

    def got_stats(t):
        remote(stats.at[t], stats.at[t], st_s.at[t], st_r.at[t], t_dev(t)).wait_recv()

    def got_kv(s):
        remote(kvs.at[s], kvs.at[s], kv_s.at[s], kv_r.at[s], s_dev(s)).wait_recv()

    def relay_q(t, c):
        return remote(
            qd.at[t, c], qd.at[t, c], rq_s.at[t, c], qd_r.at[t, c], t_dev(near_t)
        )

    def relay_kv(s):
        return remote(kvs.at[s], kvs.at[s], rkv_s.at[s], kv_r.at[s], s_dev(near_s))

    def dq_copy(t):
        return remote(dq_out.at[t], dq_in.at[me_t], dq_s.at[t], dq_r.at[me_t], t_dev(t))

    def send_g(s, i):
        g_out[s, i] = dv[s].astype(BF16) if i else (dk[s] * scale).astype(BF16)
        remote(
            g_out.at[s, i], g_in.at[me_s, i], g_s.at[s, i], g_r.at[me_s, i], s_dev(s)
        ).start()

    tile(me_t, me_s)
    for s in far_s:
        got_kv(s)
        relay_kv(s).start()
    got_kv(near_s)
    tile(me_t, near_s)
    for c in range(2):
        for t in far_t:
            got_q(t, c)
            relay_q(t, c).start()
        if c == 0:
            for s in far_s:
                tile(me_t, s)
            for c2 in range(2):
                got_q(near_t, c2)
            got_stats(near_t)
    for s in [me_s, near_s] + far_s:
        tile(near_t, s)
    for t in far_t:
        got_stats(t)
        for s in [me_s, near_s] + far_s:
            tile(t, s)
    for s in diag_s:
        got_kv(s)
        for t in [near_t] + far_t + [me_t]:
            tile(t, s)
    dq_out[near_t] = (dq_acc[near_t] * scale).astype(BF16)
    dq_copy(near_t).start()
    for n, t in enumerate(diag_t):
        for c in range(2):
            got_q(t, c)
        got_stats(t)
        for s in far_s + diag_s + [near_s]:
            tile(t, s)
            if n == len(diag_t) - 1:
                send_g(s, 0)
        if n == len(diag_t) - 1:
            for s in far_s + diag_s + [near_s]:
                send_g(s, 1)
        tile(t, me_s)
        dq_out[t] = (dq_acc[t] * scale).astype(BF16)
        remote(dq_out.at[t], dq_via.at[t], dq_s.at[t], via_r.at[t], t_dev(near_t)).start()
    for t in far_t:
        remote(dq_out.at[t], dq_via.at[t], dq_s.at[t], via_r.at[t], t_dev(near_t)).wait_recv()
        dq_out[t] = (dq_acc[t] * scale + dq_via[t].astype(F32)).astype(BF16)
        dq_copy(t).start()

    def reduce_g(i):
        total = dv[me_s] if i else dk[me_s] * scale
        for s in s_peers:
            remote(
                g_in.at[s, i], g_in.at[s, i], g_s.at[s, i], g_r.at[s, i], s_dev(s)
            ).wait_recv()
            total += g_in[s, i].astype(F32)
        tp_own[i] = total.astype(BF16)
        for p in tp_peers:
            remote(
                tp_own.at[i], tp_in.at[tp, i], tp_s.at[p, i], tp_r.at[tp, i], tp_dev(p)
            ).start()
        tp_in[tp, i] = tp_own[i]

    def gather_g(i):
        for p in tp_peers:
            remote(
                tp_in.at[p, i], tp_in.at[p, i], tp_s.at[p, i], tp_r.at[p, i], tp_dev(p)
            ).wait_recv()
        for g in range(KV_HEADS):
            owners = [p for p in range(tp_n) if p * heads // per_key == g]
            half = tp_in[owners[0], i]
            if len(owners) > 1:
                total = half.astype(F32)
                for p in owners[1:]:
                    total += tp_in[p, i].astype(F32)
                half = total.astype(BF16)
            kv_ref[:, pl.ds((i * KV_HEADS + g) * HEAD_DIM, HEAD_DIM)] = half

    reduce_g(0)
    load.wait()
    gather_g(0)
    part = a2_own.shape[1]
    cut = a2_own.shape[2]
    key_half = kv_ref[:, 0 : KV_HEADS * HEAD_DIM]
    w_scale = 1.0 / math.sqrt(src_total)
    partial = dot_tn(key_half, src[...]) * w_scale
    for o in range(key_m):
        for i in range(key_n):
            low = (o * key_n + i) * part
            block = partial[low : low + part].astype(BF16)
            a_out[i, o] = block[:, :cut]
            b_out[o, i] = block[:, cut:]
    for i in i_peers:
        remote(a_out.at[i], a_in.at[me_i], a_s.at[i], a_r.at[me_i], i_dev(i)).start()
    for o in o_peers:
        remote(b_out.at[o], b_in.at[me_o], b_s.at[o], b_r.at[me_o], o_dev(o)).start()

    reduce_g(1)
    gather_g(1)
    dq_total = dq_acc[me_t] * scale
    for t in [near_t] + far_t:
        remote(dq_in.at[t], dq_in.at[t], dq_s.at[t], dq_r.at[t], t_dev(t)).wait_recv()
        dq_total += dq_in[t].astype(F32)
    for h in range(heads):
        low = h % per_chunk * rows
        dq_ref[:, h * HEAD_DIM : (h + 1) * HEAD_DIM] = dq_total[h // per_chunk, low : low + rows]

    total = b_out[me_o].astype(F32)
    for o in o_peers:
        remote(b_in.at[o], b_in.at[o], b_s.at[o], b_r.at[o], o_dev(o)).wait_recv()
        total += b_in[o].astype(F32)
    b2_own[...] = total
    b2_out[...] = total.astype(BF16)
    for i in i_peers:
        remote(b2_out.at[i], b2_in.at[me_i], b2_s.at[i], b2_r.at[me_i], i_dev(i)).start()
    total = a_out[me_i].astype(F32)
    for i in i_peers:
        remote(a_in.at[i], a_in.at[i], a_s.at[i], a_r.at[i], i_dev(i)).wait_recv()
        total += a_in[i].astype(F32)
    a2_own[...] = total
    a2_out[...] = total.astype(BF16)
    for o in o_peers:
        remote(a2_out.at[o], a2_in.at[me_o], a2_s.at[o], a2_r.at[me_o], o_dev(o)).start()
    total = b2_own[me_i]
    for i in i_peers:
        remote(b2_in.at[i], b2_in.at[i], b2_s.at[i], b2_r.at[i], i_dev(i)).wait_recv()
        total += b2_in[i].astype(F32)
    kg_ref[:, cut:] = total
    total = a2_own[me_o]
    for o in o_peers:
        remote(a2_in.at[o], a2_in.at[o], a2_s.at[o], a2_r.at[o], o_dev(o)).wait_recv()
        total += a2_in[o].astype(F32)
    kg_ref[:, :cut] = total

    for t in far_t + [near_t]:
        for c in range(2):
            remote(qd.at[t, c], qd.at[t, c], qd_s.at[t, c], qd_r.at[t, c], t_dev(t)).wait_send()
    for t in far_t:
        for c in range(2):
            relay_q(t, c).wait_send()
    for t in t_peers:
        remote(stats.at[t], stats.at[t], st_s.at[t], st_r.at[t], t_dev(t)).wait_send()
        remote(dq_out.at[t], dq_in.at[t], dq_s.at[t], dq_r.at[t], t_dev(t)).wait_send()
    for s in far_s + [near_s]:
        remote(kvs.at[s], kvs.at[s], kv_s.at[s], kv_r.at[s], s_dev(s)).wait_send()
    for s in far_s:
        relay_kv(s).wait_send()
    for s in s_peers:
        for i in range(2):
            remote(
                g_out.at[s, i], g_in.at[s, i], g_s.at[s, i], g_r.at[s, i], s_dev(s)
            ).wait_send()
    for i in i_peers:
        remote(a_out.at[i], a_in.at[i], a_s.at[i], a_r.at[i], i_dev(i)).wait_send()
        remote(b2_out.at[i], b2_in.at[i], b2_s.at[i], b2_r.at[i], i_dev(i)).wait_send()
    for o in o_peers:
        remote(b_out.at[o], b_in.at[o], b_s.at[o], b_r.at[o], o_dev(o)).wait_send()
        remote(a2_out.at[o], a2_in.at[o], a2_s.at[o], a2_r.at[o], o_dev(o)).wait_send()
    for p in tp_peers:
        for i in range(2):
            remote(
                tp_own.at[i], tp_in.at[p, i], tp_s.at[p, i], tp_r.at[p, i], tp_dev(p)
            ).wait_send()


def finish_kernel(
    kv_hbm, kw_hbm, vw_hbm, dq_hbm, kg_hbm, out_ref, dq_out, kg_out,
    kv, kw, vw, dq, kg, buf, in_sems, w_sems, out_sems, pass_sems,
):
    half = kw.shape[1]
    width = buf.shape[2]
    count = buf.shape[0]
    load = pltpu.make_async_copy(kv_hbm, kv, in_sems.at[0])
    load.start()
    loads = []
    for n in range(count):
        cols = pl.ds(n * width, width)
        loads.append(
            [
                pltpu.make_async_copy(ref.at[cols], to.at[cols], w_sems.at[n, i])
                for i, (ref, to) in enumerate(((kw_hbm, kw), (vw_hbm, vw)))
            ]
        )
        for copy in loads[n]:
            copy.start()
    dq_in = pltpu.make_async_copy(dq_hbm, dq, in_sems.at[1])
    kg_in = pltpu.make_async_copy(kg_hbm, kg, in_sems.at[2])
    dq_in.start()
    kg_in.start()
    load.wait()
    copies = []
    for n in range(count):
        cols = slice(n * width, (n + 1) * width)
        for copy in loads[n]:
            copy.wait()
        buf[n] = dot_nt(kv[:, :half], kw[cols]) + dot_nt(kv[:, half:], vw[cols])
        copies.append(
            pltpu.make_async_copy(
                buf.at[n], out_ref.at[:, pl.ds(n * width, width)], out_sems.at[n]
            )
        )
        copies[n].start()
    dq_in.wait()
    copies.append(pltpu.make_async_copy(dq, dq_out, pass_sems.at[0]))
    copies[-1].start()
    kg_in.wait()
    copies.append(pltpu.make_async_copy(kg, kg_out, pass_sems.at[1]))
    copies[-1].start()
    for copy in copies:
        copy.wait()


def shards(
    tgt_n, src_n, tp_n,
    queries, attn_out, out_grad, row_lse, source, saved_keys, saved_values, key_weight, value_weight
):
    heads = row_lse.shape[1]
    rows, width = queries.shape
    src_rows, columns = source.shape
    kv_width = KV_HEADS * HEAD_DIM
    sp_n = tgt_n * src_n
    part = kv_width // sp_n
    key_n, key_m = src_n, tgt_n
    chunks = math.gcd(heads, 2)
    stacked = heads // chunks * rows
    cut = (2 * columns // 3 + 127) // 128 * 128
    rest = columns - cut
    dma = pltpu.SemaphoreType.DMA
    vmem = pl.BlockSpec(memory_space=pltpu.VMEM)
    scratch = [
        pltpu.VMEM((tgt_n, 2, rows, width), BF16),
        pltpu.VMEM((tgt_n, chunks, 8, stacked), F32),
        pltpu.VMEM((src_n, 2, src_rows, HEAD_DIM), BF16),
        pltpu.VMEM((src_n, src_rows, HEAD_DIM), F32),
        pltpu.VMEM((src_n, src_rows, HEAD_DIM), F32),
        pltpu.VMEM((tgt_n, chunks, stacked, HEAD_DIM), F32),
        pltpu.VMEM((tgt_n, chunks, stacked, HEAD_DIM), BF16),
        pltpu.VMEM((tgt_n, chunks, stacked, HEAD_DIM), BF16),
        pltpu.VMEM((tgt_n, chunks, stacked, HEAD_DIM), BF16),
        pltpu.VMEM((src_n, 2, src_rows, HEAD_DIM), BF16),
        pltpu.VMEM((src_n, 2, src_rows, HEAD_DIM), BF16),
        pltpu.VMEM((2, src_rows, HEAD_DIM), BF16),
        pltpu.VMEM((tp_n, 2, src_rows, HEAD_DIM), BF16),
        pltpu.VMEM((src_rows, columns), BF16),
        pltpu.VMEM((key_n, key_m, part, cut), BF16),
        pltpu.VMEM((key_n, key_m, part, cut), BF16),
        pltpu.VMEM((key_m, part, cut), F32),
        pltpu.VMEM((key_m, part, cut), BF16),
        pltpu.VMEM((key_m, part, cut), BF16),
        pltpu.VMEM((key_m, key_n, part, rest), BF16),
        pltpu.VMEM((key_m, key_n, part, rest), BF16),
        pltpu.VMEM((key_n, part, rest), F32),
        pltpu.VMEM((key_n, part, rest), BF16),
        pltpu.VMEM((key_n, part, rest), BF16),
        dma,
    ]
    for shape in (
        (tgt_n, 2), (tgt_n, 2), (tgt_n, 2), (tgt_n,), (tgt_n,),
        (src_n,), (src_n,), (src_n,), (tgt_n,), (tgt_n,), (tgt_n,), (src_n, 2), (src_n, 2),
        (tp_n, 2), (tp_n, 2), (key_n,), (key_n,), (key_m,), (key_m,),
        (key_m,), (key_m,), (key_n,), (key_n,),
    ):
        scratch.append(dma(shape))
    query_grad, kv_half, key_grad = pl.pallas_call(
        functools.partial(kernel, tgt_n, src_n, key_n, tp_n, src_rows * sp_n),
        out_shape=(
            jax.ShapeDtypeStruct((rows, width), F32),
            jax.ShapeDtypeStruct((src_rows, 2 * kv_width), BF16),
            jax.ShapeDtypeStruct((part, columns), F32),
        ),
        in_specs=[vmem] * 6 + [pl.BlockSpec(memory_space=pl.ANY)],
        out_specs=(vmem, vmem, vmem),
        scratch_shapes=scratch,
        compiler_params=pltpu.CompilerParams(
            collective_id=0, has_side_effects=True, vmem_limit_bytes=60 * 2**20
        ),
        name="attention_grads",
    )(queries, attn_out, out_grad, row_lse.T, saved_keys, saved_values, source)
    local_columns = key_weight.shape[0]
    blocks = local_columns // math.gcd(local_columns, 256)
    hbm = pl.BlockSpec(memory_space=pl.ANY)
    source_grad, query_grad, key_grad = pl.pallas_call(
        finish_kernel,
        out_shape=(
            jax.ShapeDtypeStruct((src_rows, local_columns), F32),
            jax.ShapeDtypeStruct((rows, width), F32),
            jax.ShapeDtypeStruct((part, columns), F32),
        ),
        in_specs=[hbm] * 5,
        out_specs=(hbm, hbm, hbm),
        scratch_shapes=[
            pltpu.VMEM((src_rows, 2 * kv_width), BF16),
            pltpu.VMEM((local_columns, kv_width), BF16),
            pltpu.VMEM((local_columns, kv_width), BF16),
            pltpu.VMEM((rows, width), F32),
            pltpu.VMEM((part, columns), F32),
            pltpu.VMEM((blocks, src_rows, local_columns // blocks), F32),
            dma((3,)),
            dma((blocks, 2)),
            dma((blocks,)),
            dma((2,)),
        ],
        compiler_params=pltpu.CompilerParams(vmem_limit_bytes=60 * 2**20),
        name="source_grads",
    )(kv_half, key_weight, value_weight, query_grad, key_grad)
    return (query_grad, source_grad, key_grad)


def solution(mesh):
    sp_n, tp_n = mesh.shape["sp"], mesh.shape["tp"]
    src_n = 2 ** (int(math.log2(sp_n)) // 2)
    in_specs = (
        P("sp", "tp"),
        P("sp", "tp"),
        P("sp", "tp"),
        P("sp", "tp"),
        P("sp", "tp"),
        P("sp", None),
        P("sp", None),
        P("tp", None),
        P("tp", None),
    )
    out_specs = (P("sp", "tp"), P("sp", "tp"), P("sp", "tp"))
    return jax.shard_map(
        functools.partial(shards, sp_n // src_n, src_n, tp_n),
        mesh=mesh, in_specs=in_specs, out_specs=out_specs, check_vma=False,
    )
```

profile of v0, /device:TPU:1, one launch (start us, length us, event | category | flops | bytes accessed | tf_op | source)
XLA Modules:
  0.0 153.1 jit_solution(202316957179721237)
XLA Ops:
  0.6 149.4 %attention_grads.1 = (f32[128,128]{1,0:T(8,128)}, bf16[512,512]{1,0:T(8,128)(2,1)}, f32[4,512]{1,0:T(4,128)}) custom-call(bf16[128,128]{1,0:T(8,128)(2,1)} %q_ref.1, bf16[128,128]{1,0:T(8,128)(2,1)} %o_ref.1, bf16[128,128]{1,0:T(8,128)(2,1)} %d_ref.1, f32[1,128]{1,0:T(1,128)} %bitcast.1, bf16[512,256]{1,0:T(8,128)(2,1)} %key_ref.1, ...), custom_call_target="tpu_custom_call" | custom-call | tf_op jit(solution)/shard_map/attention_grads/pallas_call | solution.py:444
  150.0 2.9 %source_grads.1 = (f32[512,512]{1,0:T(8,128)}, f32[128,128]{1,0:T(8,128)}, f32[4,512]{1,0:T(4,128)}) custom-call(bf16[512,512]{1,0:T(8,128)(2,1)} %get-tuple-element.9.kv_hbm, bf16[512,256]{1,0:T(8,128)(2,1)} %kw_hbm.1, bf16[512,256]{1,0:T(8,128)(2,1)} %vw_hbm.1, f32[128,128]{1,0:T(8,128)} %get-tuple-element.10.dq_hbm, f32[4,512]{1,0:T(4,128)} %get-tuple-element.11.kg_hbm), custom_call_target="tpu_custom_call" | custom-call | tf_op jit(solution)/shard_map/source_grads/pallas_call | solution.py:462
where the time goes:
time: 154 us; the launch traced here: 153 us
  Pallas kernels  152 us (99%)
    pallas_call x1, Pallas kernels, shards(): pl.pallas_call(functools.partial(kernel, tgt_n, src_n, key_n, tp_n, src_r...  149 us

commit v1 on v0

v1 whole, which is shorter than its diff:
```python
import functools
import math

import jax
import jax.numpy as jnp
from jax import lax
from jax.experimental import pallas as pl
from jax.experimental.pallas import tpu as pltpu
from jax.sharding import PartitionSpec as P

KV_HEADS = 2
HEAD_DIM = 128
Y_N = 4
LOG2E = 1.0 / math.log(2.0)
MESH = pl.DeviceIdType.MESH
F32 = jnp.float32
BF16 = jnp.bfloat16


def dot_nt(left, right, precision=None):
    return lax.dot_general(
        left, right, (((1,), (1,)), ((), ())), preferred_element_type=F32, precision=precision
    )


def dot_tn(left, right):
    return lax.dot_general(left, right, (((0,), (0,)), ((), ())), preferred_element_type=F32)


def dot_nn(left, right):
    return jnp.dot(left, right, preferred_element_type=F32)


def kernel(
    y_n, z_n, tp_n, src_total,
    q_ref, o_ref, d_ref, lse_ref, key_ref, value_ref, source_ref,
    dq_ref, kv_ref, kg_ref,
    qd, stats, kvs, acc, dq_acc, dq_out, dq_in, pair_out, pair_in, g_own, g_out, g_in, tp_in,
    src, ky_out, ky_in, z_own, z_out, z_in,
    copy_sem, q_s, q_r, k_s, k_r, kf_s, kf_r, dq_s, dq_r, p_s, p_r, g_s, g_r, t_s, t_r, tf_s, tf_r,
    ky_s, ky_r, z_s, z_r,
):
    sp = lax.axis_index("sp")
    tp = lax.axis_index("tp")
    z, y = sp // y_n, sp % y_n
    x, c = tp // 2, tp % 2
    x_n = tp_n // 2
    per_key = tp_n // KV_HEADS
    key_col = pl.multiple_of(tp // per_key * HEAD_DIM, HEAD_DIM)
    half = z_n // 2
    rows = q_ref.shape[0]
    src_rows = key_ref.shape[0]
    hr = src_rows // 2
    scale = 1.0 / math.sqrt(HEAD_DIM)

    def zd(k):
        return {"sp": lax.rem(z + k + z_n, z_n) * y_n + y, "tp": tp}

    def yd(k):
        return {"sp": z * y_n + lax.rem(y + k + y_n, y_n), "tp": tp}

    def xd(k):
        return {"sp": sp, "tp": lax.rem(x + k + x_n, x_n) * 2 + c}

    partner = {"sp": sp, "tp": x * 2 + 1 - c}

    def remote(source, target, send, recv, device):
        return pltpu.make_async_remote_copy(
            src_ref=source, dst_ref=target, send_sem=send, recv_sem=recv,
            device_id=device, device_id_type=MESH,
        )

    load = pltpu.make_async_copy(source_ref, src, copy_sem)
    load.start()
    barrier = pltpu.get_barrier_semaphore()
    greet = [zd(1), zd(-1)] + [yd(k) for k in range(1, y_n)]
    greet += [xd(k) for k in range(1, x_n)] + [partner]
    for device in greet:
        pl.semaphore_signal(barrier, inc=1, device_id=device, device_id_type=MESH)
    prod = d_ref[...].astype(F32) * o_ref[...].astype(F32)
    delta = dot_nt(jnp.ones((8, HEAD_DIM), F32), prod, lax.Precision.HIGHEST)
    for way in range(2):
        stats[way, 0, 0:1, :] = lse_ref[0:1, :] * LOG2E
        stats[way, 0, 1:2, :] = delta[0:1, :]
    kvs[0, 0] = key_ref[:, pl.ds(key_col, HEAD_DIM)]
    kvs[0, 1] = value_ref[:, pl.ds(key_col, HEAD_DIM)]
    pl.semaphore_wait(barrier, len(greet))

    steps = [zd(1), zd(-1)]

    def q_copy(way, d, i):
        if i == 2:
            source, target = stats.at[way, d], stats.at[way, d + 1]
        else:
            source = (q_ref, d_ref)[i] if d == 0 else qd.at[way, d, i]
            target = qd.at[way, d + 1, i]
        return remote(source, target, q_s.at[way, d, i], q_r.at[way, d + 1, i], steps[way])

    def pieces(way, d):
        if d < half:
            return (2, 0, 1)
        return (2, 0) if way == 0 else (1,)

    def relay(d):
        for i in (2, 0, 1):
            for way in range(2):
                if d > 0 and i in pieces(way, d):
                    q_copy(way, d - 1, i).wait_recv()
                if d < half and i in pieces(way, d + 1):
                    q_copy(way, d, i).start()

    def k_copy(k):
        return remote(
            kvs.at[0, c], kvs.at[y_n - k, c], k_s.at[k], k_r.at[y_n - k], yd(k)
        )

    lo, hi = pl.ds(0, hr), pl.ds(hr, hr)
    k_relays = (
        remote(kvs.at[3, c, lo], kvs.at[2, c, lo], k_s.at[0], k_r.at[0], yd(1)),
        remote(kvs.at[1, c, hi], kvs.at[2, c, hi], k_s.at[2], k_r.at[2], yd(-1)),
    )

    def k_pass(k, role):
        return remote(kvs.at[k, role], kvs.at[k, role], kf_s.at[k], kf_r.at[k], partner)

    def got_sides():
        for k in (3, 1):
            k_copy(y_n - k).wait_recv()
            k_relays[0 if k == 3 else 1].start()
            k_pass(k, c).start()
        for k in (3, 1):
            k_pass(k, 1 - c).wait_recv()

    def got_across():
        for copy in k_relays:
            copy.wait_recv()
        k_pass(2, c).start()
        k_pass(2, 1 - c).wait_recv()

    seen = set()

    def add(ref, key, value):
        if key in seen:
            ref[...] += value
        else:
            ref[...] = value
            seen.add(key)

    def tile(d, blocks):
        if d == 0:
            q, g = q_ref[...], d_ref[...]
            lse, delta = stats[0, 0, 0:1, :], stats[0, 0, 1:2, :]
        elif d == half:
            q, g = qd[0, d, 0], qd[1, d, 1]
            lse, delta = stats[0, d, 0:1, :], stats[0, d, 1:2, :]
        else:
            q = jnp.concatenate([qd[0, d, 0], qd[1, d, 0]], axis=0)
            g = jnp.concatenate([qd[0, d, 1], qd[1, d, 1]], axis=0)
            lse = jnp.concatenate([stats[0, d, 0:1, :], stats[1, d, 0:1, :]], axis=1)
            delta = jnp.concatenate([stats[0, d, 1:2, :], stats[1, d, 1:2, :]], axis=1)
        for s in blocks:
            k, v = kvs[s, 0], kvs[s, 1]
            probs = jnp.exp2(dot_nt(k, q) * (scale * LOG2E) - lse)
            dscores = (probs * (dot_nt(v, g) - delta)).astype(BF16)
            add(acc.at[1, s], ("v", s), dot_nn(probs.astype(BF16), g))
            add(acc.at[0, s], ("k", s), dot_nn(dscores, q))
            add(dq_acc.at[d, pl.ds(0, q.shape[0])], ("q", d), dot_tn(dscores, k))

    def dq_copy(way, d):
        return remote(
            dq_out.at[d, pl.ds(way * rows, rows)], dq_in.at[d, pl.ds(way * rows, rows)],
            dq_s.at[d, way], dq_r.at[d, way], zd(d if way else -d),
        )

    def ways(d):
        return range(1 if d == half else 2)

    def send_dq(d):
        span = pl.ds(0, rows * len(ways(d)))
        dq_out[d, span] = (dq_acc[d, span] * scale).astype(BF16)
        for way in ways(d):
            dq_copy(way, d).start()

    mine, other = pl.ds(pl.multiple_of(c * hr, hr), hr), pl.ds(pl.multiple_of((1 - c) * hr, hr), hr)

    def pair_copy(i, k):
        return remote(pair_out.at[i, k], pair_in.at[i, k], p_s.at[i, k], p_r.at[i, k], partner)

    def send_pair(k):
        for i in range(2):
            part = acc[i, k, other, :]
            pair_out[i, k] = (part if i else part * scale).astype(BF16)
            pair_copy(i, k).start()

    def g_copy(i, k):
        return remote(
            g_out.at[i, k], g_in.at[i, y_n - k], g_s.at[i, k], g_r.at[i, y_n - k], yd(k)
        )

    order = (2, 1, 3, 0)
    relay(0)
    for k in (1, 3):
        k_copy(k).start()
    tile(0, (0,))
    relay(1)
    if half > 1:
        tile(1, (0,))
    got_sides()
    late = {0: (0,), 1: (0,)}
    for d in range(2, half):
        relay(d)
        if d == 2:
            tile(0, (1, 3))
            tile(1, (1, 3))
            tile(2, (0, 1, 3))
            got_across()
        elif d == 3:
            tile(3, (0, 1, 2, 3))
            tile(0, (2,))
            tile(1, (2,))
            tile(2, (2,))
        else:
            tile(d, (0, 1, 2, 3))
    if half == 2:
        tile(0, (1, 3))
        tile(1, (1, 3))
        got_across()
        tile(0, (2,))
        tile(1, (2,))
    elif half == 3:
        tile(0, (2,))
        tile(1, (2,))
        tile(2, (2,))
    relay(half)
    for d in range(1, half):
        send_dq(d)
    for k in order:
        tile(half, (k,))
        send_pair(k)
    send_dq(half)

    def reduce_pair(i):
        for k in order:
            pair_copy(i, k).wait_recv()
            part = acc[i, k, mine, :]
            total = (part if i else part * scale) + pair_in[i, k].astype(F32)
            if k:
                g_out[i, k] = total.astype(BF16)
                g_copy(i, k).start()
            else:
                g_own[i] = total

    def tp_copy(i, k):
        return remote(tp_in.at[i, x, c], tp_in.at[i, x, c], t_s.at[i, k], t_r.at[i, x], xd(k))

    def tp_got(i, k):
        other_x = lax.rem(x + k, x_n)
        return remote(
            tp_in.at[i, other_x, c], tp_in.at[i, other_x, c], t_s.at[i, k], t_r.at[i, other_x], xd(k)
        )

    def tp_pass(i, k, role):
        at = lax.rem(x + k, x_n)
        return remote(
            tp_in.at[i, at, role], tp_in.at[i, at, role], tf_s.at[i, at], tf_r.at[i, at], partner
        )

    def reduce_sites(i):
        total = g_own[i]
        for k in range(1, y_n):
            g_copy(i, y_n - k).wait_recv()
            total += g_in[i, k].astype(F32)
        tp_in[i, x, c] = total.astype(BF16)
        for k in range(1, x_n):
            tp_copy(i, k).start()
        tp_pass(i, 0, c).start()

    def gather_heads(i):
        for k in range(1, x_n):
            tp_got(i, k).wait_recv()
            tp_pass(i, k, c).start()
        for k in range(x_n):
            tp_pass(i, k, 1 - c).wait_recv()
        chips = x_n // KV_HEADS
        for g in range(KV_HEADS):
            for r in range(2):
                total = tp_in[i, g * chips, r]
                if chips > 1:
                    total = total.astype(F32)
                    for p in range(1, chips):
                        total += tp_in[i, g * chips + p, r].astype(F32)
                col = (i * KV_HEADS + g) * HEAD_DIM
                kv_ref[r * hr : (r + 1) * hr, col : col + HEAD_DIM] = total.astype(BF16)

    reduce_pair(0)
    reduce_pair(1)
    reduce_sites(0)
    load.wait()
    reduce_sites(1)
    gather_heads(0)

    width = KV_HEADS * HEAD_DIM
    part = width // (y_n * z_n)
    to = lax.broadcasted_iota(jnp.int32, (width, width), 1)
    at = lax.broadcasted_iota(jnp.int32, (width, width), 0)
    home = (to % (z_n * part)) // part * (y_n * part) + to // (z_n * part) * part + to % part
    pick = jnp.where(at == home, 1.0, 0.0).astype(BF16)
    key_half = dot_nn(kv_ref[:, 0:width], pick).astype(BF16)
    partial = dot_tn(key_half, src[...]) * (1.0 / math.sqrt(src_total))
    for k in range(y_n):
        ky_out[k] = partial[k * z_n * part : (k + 1) * z_n * part].astype(BF16)

    def ky_copy(k):
        return remote(
            ky_out.at[lax.rem(y + k, y_n)], ky_in.at[y_n - k], ky_s.at[k], ky_r.at[y_n - k], yd(k)
        )

    for k in (2, 1, 3):
        ky_copy(k).start()

    gather_heads(1)

    total = ky_out[y].astype(F32)
    for k in range(1, y_n):
        ky_copy(y_n - k).wait_recv()
        total += ky_in[k].astype(F32)
    for k in range(z_n):
        z_own[k] = total[k * part : (k + 1) * part]
        z_out[k] = total[k * part : (k + 1) * part].astype(BF16)

    def z_copy(k):
        return remote(
            z_out.at[lax.rem(z + k, z_n)], z_in.at[z_n - k], z_s.at[k], z_r.at[z_n - k], zd(k)
        )

    far = sorted(range(1, z_n), key=lambda k: -min(k, z_n - k))
    for k in far:
        z_copy(k).start()

    total = dq_acc[0, pl.ds(0, rows)] * scale
    for d in range(1, half + 1):
        for way in ways(d):
            dq_copy(way, d).wait_recv()
            total += dq_in[d, pl.ds(way * rows, rows)].astype(F32)
    dq_ref[...] = total

    total = z_own[z]
    for k in reversed(far):
        z_copy(z_n - k).wait_recv()
        total += z_in[k].astype(F32)
    kg_ref[...] = total

    for d in range(half):
        for way in range(2):
            for i in pieces(way, d + 1):
                q_copy(way, d, i).wait_send()
    for d in range(1, half + 1):
        for way in ways(d):
            dq_copy(way, d).wait_send()
    for k in (1, 3):
        k_copy(k).wait_send()
    for copy in k_relays:
        copy.wait_send()
    for k in range(1, y_n):
        k_pass(k, c).wait_send()
        ky_copy(k).wait_send()
    for i in range(2):
        for k in range(y_n):
            pair_copy(i, k).wait_send()
            if k:
                g_copy(i, k).wait_send()
        for k in range(x_n):
            tp_pass(i, k, c).wait_send()
            if k:
                tp_copy(i, k).wait_send()
    for k in far:
        z_copy(k).wait_send()


def finish_kernel(
    kv_hbm, kw_hbm, vw_hbm, dq_hbm, kg_hbm, out_ref, dq_out, kg_out,
    kv, kw, vw, dq, kg, buf, in_sems, w_sems, out_sems, pass_sems,
):
    half = kw.shape[1]
    width = buf.shape[2]
    count = buf.shape[0]
    load = pltpu.make_async_copy(kv_hbm, kv, in_sems.at[0])
    load.start()
    loads = []
    for n in range(count):
        cols = pl.ds(n * width, width)
        loads.append(
            [
                pltpu.make_async_copy(ref.at[cols], to.at[cols], w_sems.at[n, i])
                for i, (ref, to) in enumerate(((kw_hbm, kw), (vw_hbm, vw)))
            ]
        )
        for copy in loads[n]:
            copy.start()
    dq_in = pltpu.make_async_copy(dq_hbm, dq, in_sems.at[1])
    kg_in = pltpu.make_async_copy(kg_hbm, kg, in_sems.at[2])
    dq_in.start()
    kg_in.start()
    load.wait()
    copies = []
    for n in range(count):
        cols = slice(n * width, (n + 1) * width)
        for copy in loads[n]:
            copy.wait()
        buf[n] = dot_nt(kv[:, :half], kw[cols]) + dot_nt(kv[:, half:], vw[cols])
        copies.append(
            pltpu.make_async_copy(
                buf.at[n], out_ref.at[:, pl.ds(n * width, width)], out_sems.at[n]
            )
        )
        copies[n].start()
    dq_in.wait()
    copies.append(pltpu.make_async_copy(dq, dq_out, pass_sems.at[0]))
    copies[-1].start()
    kg_in.wait()
    copies.append(pltpu.make_async_copy(kg, kg_out, pass_sems.at[1]))
    copies[-1].start()
    for copy in copies:
        copy.wait()

def shards(
    y_n, z_n, tp_n,
    queries, attn_out, out_grad, row_lse, source, saved_keys, saved_values, key_weight, value_weight
):
    rows, width = queries.shape
    src_rows, columns = source.shape
    kv_width = KV_HEADS * HEAD_DIM
    sp_n = y_n * z_n
    part = kv_width // sp_n
    half = z_n // 2
    x_n = tp_n // 2
    hr = src_rows // 2
    dma = pltpu.SemaphoreType.DMA
    vmem = pl.BlockSpec(memory_space=pltpu.VMEM)
    scratch = [
        pltpu.VMEM((2, half + 1, 2, rows, width), BF16),
        pltpu.VMEM((2, half + 1, 2, rows), F32),
        pltpu.VMEM((y_n, 2, src_rows, HEAD_DIM), BF16),
        pltpu.VMEM((2, y_n, src_rows, HEAD_DIM), F32),
        pltpu.VMEM((half + 1, 2 * rows, HEAD_DIM), F32),
        pltpu.VMEM((half + 1, 2 * rows, HEAD_DIM), BF16),
        pltpu.VMEM((half + 1, 2 * rows, HEAD_DIM), BF16),
        pltpu.VMEM((2, y_n, hr, HEAD_DIM), BF16),
        pltpu.VMEM((2, y_n, hr, HEAD_DIM), BF16),
        pltpu.VMEM((2, hr, HEAD_DIM), F32),
        pltpu.VMEM((2, y_n, hr, HEAD_DIM), BF16),
        pltpu.VMEM((2, y_n, hr, HEAD_DIM), BF16),
        pltpu.VMEM((2, x_n, 2, hr, HEAD_DIM), BF16),
        pltpu.VMEM((src_rows, columns), BF16),
        pltpu.VMEM((y_n, z_n * part, columns), BF16),
        pltpu.VMEM((y_n, z_n * part, columns), BF16),
        pltpu.VMEM((z_n, part, columns), F32),
        pltpu.VMEM((z_n, part, columns), BF16),
        pltpu.VMEM((z_n, part, columns), BF16),
        dma,
    ]
    for shape in (
        (2, half + 1, 3), (2, half + 1, 3), (y_n,), (y_n,), (y_n,), (y_n,), (half + 1, 2), (half + 1, 2),
        (2, y_n), (2, y_n), (2, y_n), (2, y_n), (2, x_n), (2, x_n), (2, x_n), (2, x_n),
        (y_n,), (y_n,), (z_n,), (z_n,),
    ):
        scratch.append(dma(shape))
    query_grad, kv_half, key_grad = pl.pallas_call(
        functools.partial(kernel, y_n, z_n, tp_n, src_rows * sp_n),
        out_shape=(
            jax.ShapeDtypeStruct((rows, width), F32),
            jax.ShapeDtypeStruct((src_rows, 2 * kv_width), BF16),
            jax.ShapeDtypeStruct((part, columns), F32),
        ),
        in_specs=[vmem] * 6 + [pl.BlockSpec(memory_space=pl.ANY)],
        out_specs=(vmem, vmem, vmem),
        scratch_shapes=scratch,
        compiler_params=pltpu.CompilerParams(
            collective_id=0, has_side_effects=True, vmem_limit_bytes=60 * 2**20
        ),
        name="attention_grads",
    )(queries, attn_out, out_grad, row_lse.T, saved_keys, saved_values, source)
    local_columns = key_weight.shape[0]
    blocks = local_columns // math.gcd(local_columns, 256)
    hbm = pl.BlockSpec(memory_space=pl.ANY)
    source_grad, query_grad, key_grad = pl.pallas_call(
        finish_kernel,
        out_shape=(
            jax.ShapeDtypeStruct((src_rows, local_columns), F32),
            jax.ShapeDtypeStruct((rows, width), F32),
            jax.ShapeDtypeStruct((part, columns), F32),
        ),
        in_specs=[hbm] * 5,
        out_specs=(hbm, hbm, hbm),
        scratch_shapes=[
            pltpu.VMEM((src_rows, 2 * kv_width), BF16),
            pltpu.VMEM((local_columns, kv_width), BF16),
            pltpu.VMEM((local_columns, kv_width), BF16),
            pltpu.VMEM((rows, width), F32),
            pltpu.VMEM((part, columns), F32),
            pltpu.VMEM((blocks, src_rows, local_columns // blocks), F32),
            dma((3,)),
            dma((blocks, 2)),
            dma((blocks,)),
            dma((2,)),
        ],
        compiler_params=pltpu.CompilerParams(vmem_limit_bytes=60 * 2**20),
        name="source_grads",
    )(kv_half, key_weight, value_weight, query_grad, key_grad)
    return (query_grad, source_grad, key_grad)


def solution(mesh):
    sp_n, tp_n = mesh.shape["sp"], mesh.shape["tp"]
    in_specs = (
        P("sp", "tp"),
        P("sp", "tp"),
        P("sp", "tp"),
        P("sp", "tp"),
        P("sp", "tp"),
        P("sp", None),
        P("sp", None),
        P("tp", None),
        P("tp", None),
    )
    out_specs = (P("sp", "tp"), P("sp", "tp"), P("sp", "tp"))
    return jax.shard_map(
        functools.partial(shards, Y_N, sp_n // Y_N, tp_n),
        mesh=mesh, in_specs=in_specs, out_specs=out_specs, check_vma=False,
    )
```

time: 154 us -> 78.5 us (0.51)
  Pallas kernels: 152 us -> 77.5 us
    pallas_call x1, Pallas kernels: 149 us -> 74.6 us  [shards(): pl.pallas_call(functools.partial(kernel, y_n, z_n, tp_n, src_rows * sp_n)...]
where the time goes in v1:
time: 78.5 us; the launch traced here: 78.3 us
  Pallas kernels  77.5 us (99%)
  between operations  0.8 us (1%)
    pallas_call x1, Pallas kernels, shards(): pl.pallas_call(functools.partial(kernel, y_n, z_n, tp_n, src_rows * sp_n)...  74.6 us
    pallas_call x1, Pallas kernels, shards(): pl.pallas_call(finish_kernel, out_shape=(jax.ShapeDtypeStruct((src_rows,...  2.94 us

profile of v1, /device:TPU:1, one launch (start us, length us, event | category | flops | bytes accessed | tf_op | source)
XLA Modules:
  0.0 78.3 jit_solution(11308408423818747045)
XLA Ops:
  0.6 74.6 %attention_grads.1 = (f32[128,128]{1,0:T(8,128)}, bf16[512,512]{1,0:T(8,128)(2,1)}, f32[4,512]{1,0:T(4,128)}) custom-call(bf16[128,128]{1,0:T(8,128)(2,1)} %q_ref.1, bf16[128,128]{1,0:T(8,128)(2,1)} %o_ref.1, bf16[128,128]{1,0:T(8,128)(2,1)} %d_ref.1, f32[1,128]{1,0:T(1,128)} %bitcast.1, bf16[512,256]{1,0:T(8,128)(2,1)} %key_ref.1, ...), custom_call_target="tpu_custom_call" | custom-call | tf_op jit(solution)/shard_map/attention_grads/pallas_call | solution.py:468
  75.2 2.9 %source_grads.1 = (f32[512,512]{1,0:T(8,128)}, f32[128,128]{1,0:T(8,128)}, f32[4,512]{1,0:T(4,128)}) custom-call(bf16[512,512]{1,0:T(8,128)(2,1)} %get-tuple-element.9.kv_hbm, bf16[512,256]{1,0:T(8,128)(2,1)} %kw_hbm.1, bf16[512,256]{1,0:T(8,128)(2,1)} %vw_hbm.1, f32[128,128]{1,0:T(8,128)} %get-tuple-element.10.dq_hbm, f32[4,512]{1,0:T(4,128)} %get-tuple-element.11.kg_hbm), custom_call_target="tpu_custom_call" | custom-call | tf_op jit(solution)/shard_map/source_grads/pallas_call | solution.py:486
